TPU v7x, 32 devices: a whole 2x2x4 slice. The times are simulated.
32 devices in a mesh: ep: 16 (over z, y, x), tp: 2 (over core).
Axes of the slice: x: 2, y: 2, z: 4, core: 2. Of those that a mesh axis runs over, the one named last changes fastest.
Arguments:
- tokens: bfloat16 [768, 2048], P('ep', 'tp'), may hold values from -12 to 12
- conv_state: bfloat16 [768, 3, 1024], P('ep', None, 'tp'), may hold values from -6 to 6
- hidden_state: float32 [768, 1024], P('ep', 'tp'), may hold values from -6 to 6
- mixer_gain: float32 [2048], replicated, may hold values from 0.1 to 1.9
- branch_weight: bfloat16 [2048, 1024], P(None, 'tp'), may hold values from -0.125 to 0.125
- gelu_weight: bfloat16 [2048, 1024], P(None, 'tp'), may hold values from -0.125 to 0.125
- conv_kernel: float32 [4, 1024], P(None, 'tp'), may hold values from -3 to 3
- recur_blocks: bfloat16 [16, 64, 64], P('tp'), may hold values from -0.75 to 0.75
- input_blocks: bfloat16 [16, 64, 64], P('tp'), may hold values from -0.75 to 0.75
- decay_rate: float32 [1024], P('tp'), may hold values from 0.002 to 0.1
- output_weight: bfloat16 [1024, 2048], P(None, 'tp'), may hold values from -0.1875 to 0.1875
- expert_gain: float32 [2048], replicated, may hold values from 0.1 to 1.9
- expert_ids: int32 [768, 2], P('ep'), may hold values from 0 to 15, as said below
- group_prob: float32 [768], P('ep'), may hold values from 0.25 to 1
- expert_logit: float32 [768, 2], P('ep'), may hold values from -4 to 4
- expert_gate: bfloat16 [16, 2048, 512], P('ep', None, 'tp'), may hold values from -0.125 to 0.125
- expert_up: bfloat16 [16, 2048, 512], P('ep', None, 'tp'), may hold values from -0.125 to 0.125
- expert_down: bfloat16 [16, 512, 2048], P('ep', 'tp'), may hold values from -0.25 to 0.25
Outputs:
- layer_out: bfloat16 [768, 2048], P('ep', 'tp')
- new_hidden: float32 [768, 1024], P('ep', 'tp')
Inputs may be any that keep to these rules, and one draw needn't show every extreme that they name: `expert_ids`: the two experts of a row are different and lie in one group of 4 consecutive experts. Within the rows of one index of ep no expert is named more than 6 times, and one expert is named exactly 6 times by the rows of every index of ep.
All inputs are finite; a program needn't handle non-finite values.
Results may differ from a plain program's by a relative error of at most 0.012.
Values may be sent and summed in bfloat16 or wider, within the bound.
A program may use at most 64 MiB of HBM per device.

v0:
```python
import jax
import jax.numpy as jnp
from jax import lax
from jax.sharding import PartitionSpec as P

EPSILON = 1e-06
RATE_SCALE = 8.0


def normalize(values, gain_row):
    squares = jnp.mean(values * values, axis=-1, keepdims=True)
    return values * lax.rsqrt(squares + EPSILON) * gain_row


def local(
    tokens,
    conv_state,
    hidden_state,
    mixer_gain,
    branch_weight,
    gelu_weight,
    conv_kernel,
    recur_blocks,
    input_blocks,
    decay_rate,
    output_weight,
    expert_gain,
    expert_ids,
    group_prob,
    expert_logit,
    expert_gate,
    expert_up,
    expert_down,
):
    whole_tokens = lax.all_gather(tokens, "tp", axis=1, tiled=True)
    normed = normalize(whole_tokens.astype(jnp.float32), mixer_gain).astype(jnp.bfloat16)
    branch = jnp.dot(normed, branch_weight, preferred_element_type=jnp.float32).astype(jnp.bfloat16)
    gelu_input = jnp.dot(normed, gelu_weight, preferred_element_type=jnp.float32).astype(
        jnp.bfloat16
    )
    window = jnp.concatenate([conv_state, branch[:, None, :]], axis=1).astype(jnp.float32)
    convolved = jnp.sum(window * conv_kernel[None], axis=1).astype(jnp.bfloat16)
    sequences, channels = convolved.shape
    blocks, block_size = (recur_blocks.shape[0], recur_blocks.shape[1])
    grouped = convolved.reshape(sequences, blocks, block_size)
    recur_pre = jnp.einsum(
        "tnc,ncd->tnd", grouped, recur_blocks, preferred_element_type=jnp.float32
    ).reshape(sequences, channels)
    input_pre = jnp.einsum(
        "tnc,ncd->tnd", grouped, input_blocks, preferred_element_type=jnp.float32
    ).reshape(sequences, channels)
    recur_gate = jax.nn.sigmoid(recur_pre)
    input_gate = jax.nn.sigmoid(input_pre)
    log_decay = -RATE_SCALE * recur_gate * decay_rate
    new_hidden = jnp.exp(log_decay) * hidden_state + jnp.sqrt(-jnp.expm1(2.0 * log_decay)) * (
        input_gate * convolved.astype(jnp.float32)
    )
    mixed_rows = (
        new_hidden * jax.nn.gelu(gelu_input.astype(jnp.float32), approximate=True)
    ).astype(jnp.bfloat16)
    mixed_whole = lax.all_gather(mixed_rows, "tp", axis=1, tiled=True)
    residual = (
        tokens.astype(jnp.float32)
        + jnp.dot(mixed_whole, output_weight, preferred_element_type=jnp.float32)
    ).astype(jnp.bfloat16)
    experts = lax.axis_size("ep")
    top_count = expert_ids.shape[1]
    capacity = 2 * max(1, sequences // experts)
    flat_ids = expert_ids.reshape(-1)
    onehot_ids = (flat_ids[:, None] == jnp.arange(experts, dtype=jnp.int32)[None, :]).astype(
        jnp.int32
    )
    earlier = jnp.cumsum(onehot_ids, axis=0) - onehot_ids
    ranking = jnp.sum(earlier * onehot_ids, axis=1)
    slot_index = flat_ids * capacity + ranking
    placing = (
        jnp.arange(experts * capacity, dtype=jnp.int32)[:, None] == slot_index[None, :]
    ).astype(jnp.float32)
    placing = jnp.sum(placing.reshape(experts * capacity, sequences, top_count), axis=2).astype(
        jnp.bfloat16
    )
    values = residual.astype(jnp.float32)
    half_width = values.shape[1]
    square_total = lax.psum(jnp.sum(values * values, axis=1), "tp")
    gain_part = lax.dynamic_slice_in_dim(
        expert_gain, lax.axis_index("tp") * half_width, half_width, 0
    )
    scaling = lax.rsqrt(square_total / (half_width * lax.axis_size("tp")) + EPSILON)
    moe_input = (values * scaling[:, None] * gain_part[None, :]).astype(jnp.bfloat16)
    outgoing = jnp.dot(placing, moe_input, preferred_element_type=jnp.float32).astype(jnp.bfloat16)
    outgoing = outgoing.reshape(experts, capacity, half_width)
    received = lax.all_gather(
        lax.all_to_all(outgoing, "ep", split_axis=0, concat_axis=0, tiled=True),
        "tp",
        axis=2,
        tiled=True,
    )
    sources, slot_count, features = received.shape
    flat_rows = received.reshape(sources * slot_count, features)
    gate_part = jnp.dot(flat_rows, expert_gate[0], preferred_element_type=jnp.float32)
    upper_part = jnp.dot(flat_rows, expert_up[0], preferred_element_type=jnp.float32)
    hidden_units = (jax.nn.silu(gate_part) * upper_part).astype(jnp.bfloat16)
    partial_value = jnp.dot(
        hidden_units, expert_down[0], preferred_element_type=jnp.float32
    ).reshape(sources, slot_count, features)
    summed = lax.psum_scatter(
        partial_value.astype(jnp.bfloat16), "tp", scatter_dimension=2, tiled=True
    )
    returned = lax.all_to_all(summed, "ep", split_axis=0, concat_axis=0, tiled=True)
    out_width = returned.shape[2]
    picked = jnp.take(returned.reshape(experts * capacity, out_width), slot_index, axis=0).reshape(
        sequences, top_count, out_width
    )
    logit_exp = jnp.exp(expert_logit)
    weights = group_prob[:, None] * logit_exp / jnp.sum(logit_exp, axis=1, keepdims=True)
    layer_out = (
        residual.astype(jnp.float32)
        + jnp.sum(weights[:, :, None] * picked.astype(jnp.float32), axis=1)
    ).astype(jnp.bfloat16)
    return (layer_out, new_hidden)


def solution(mesh):
    return jax.shard_map(
        local,
        mesh=mesh,
        in_specs=(
            P("ep", "tp"),
            P("ep", None, "tp"),
            P("ep", "tp"),
            P(),
            P(None, "tp"),
            P(None, "tp"),
            P(None, "tp"),
            P("tp", None, None),
            P("tp", None, None),
            P("tp"),
            P(None, "tp"),
            P(),
            P("ep", None),
            P("ep"),
            P("ep", None),
            P("ep", None, "tp"),
            P("ep", None, "tp"),
            P("ep", "tp", None),
        ),
        out_specs=(P("ep", "tp"), P("ep", "tp")),
        check_vma=False,
    )
```

profile of v0, /device:TPU:0, one launch (start us, length us, event | category | flops | bytes accessed | tf_op | source)
XLA Modules:
  0.0 81.5 jit_solution(5412062372316779908)
XLA Ops:
  7.3 2.4 %all_gather.9 = bf16[48,2048]{1,0:T(8,128)(2,1)S(1)} all-gather(bf16[48,1024]{1,0:T(8,128)(2,1)} %param.18), channel_id=1, replica_groups=mesh['ep'=16,'tp'=2] {'tp'}, dimensions={1}, use_global_device_ids=true | all-gather | bytes 294912 | tf_op jit(solution)/shard_map/all_gather | solution.py:35
  9.7 0.1 fusion.17
  9.8 2.2 %fusion.12 = bf16[48,1,512]{2,0,1:T(8,128)(2,1)S(1)} fusion(bf16[2048,512]{1,0:T(8,128)(2,1)} %param.22, bf16[48,2048]{1,0:T(8,128)(2,1)S(1)} %all_gather.9, f32[2048]{0:T(1024)} %param.21, f32[48]{0:T(128)S(1)} %add_rsqrt_fusion.1), kind=kOutput, calls=%fused_computation.21 | convolution fusion | flops 101081088 | bytes 2351296 | tf_op jit(solution)/shard_map/dot_general | solution.py:37
  12.1 0.1 convert_element_type.75
  12.2 0.2 fusion.7
  12.5 0.1 div.37
  12.6 0.2 fusion.3
  12.9 0.1 div.39
  13.2 2.2 %fusion.28 = bf16[48,512]{1,0:T(8,128)(2,1)S(1)} fusion(f32[48,512]{1,0:T(8,128)S(1)} %multiply_add_fusion, bf16[2048,512]{1,0:T(8,128)(2,1)} %param.23, bf16[48,2048]{1,0:T(8,128)(2,1)S(1)} %all_gather.9, f32[2048]{0:T(1024)S(1)} %copy-done.5, f32[48]{0:T(128)S(1)} %add_rsqrt_fusion.1), kind=kOutput, calls=%fused_computation.46 | convolution fusion | flops 101351424 | bytes 2449600 | tf_op jit(solution)/shard_map/dot_general | solution.py:38
  15.4 1.9 %all_gather.10 = bf16[48,1024]{1,0:T(8,128)(2,1)S(1)} all-gather(bf16[48,512]{1,0:T(8,128)(2,1)S(1)} %fusion.28), channel_id=1, replica_groups=mesh['ep'=16,'tp'=2] {'tp'}, dimensions={1}, use_global_device_ids=true | all-gather | bytes 147456 | tf_op jit(solution)/shard_map/all_gather | solution.py:61
  17.3 0.6 multiply_reduce_fusion.2
  17.9 2.5 %psum.7 = f32[48]{0:T(128)S(1)} all-reduce(f32[48]{0:T(128)S(1)} %get-tuple-element.4), channel_id=1, replica_groups=mesh['ep'=16,'tp'=2] {'tp'}, use_global_device_ids=true, to_apply=%region_7.8 | all-reduce | flops 48 | bytes 384 | tf_op jit(solution)/shard_map/psum | solution.py:84
  20.5 0.1 reshape.111
  20.7 0.1 reduce_window_sum.11
  20.8 0.2 select_reduce_fusion
  21.0 0.1 reduce_sum.71
  21.3 0.3 convolution_convert_fusion.1
  21.7 18.2 %all_to_all.10 = bf16[16,6,1024]{2,1,0:T(8,128)(2,1)S(1)} all-to-all(bf16[16,6,1024]{2,1,0:T(8,128)(2,1)S(1)} %reshape.112), channel_id=1, replica_groups=mesh['ep'=16,'tp'=2] {'ep'}, dimensions={0} | all-to-all | bytes 393216 | tf_op jit(solution)/shard_map/all_to_all | solution.py:93
  39.9 2.2 %all_gather.11 = bf16[16,6,2048]{2,1,0:T(8,128)(2,1)S(1)} all-gather(bf16[16,6,1024]{2,1,0:T(8,128)(2,1)S(1)} %all_to_all.10), channel_id=1, replica_groups=mesh['ep'=16,'tp'=2] {'tp'}, dimensions={2}, use_global_device_ids=true | all-gather | bytes 589824 | tf_op jit(solution)/shard_map/all_gather | solution.py:92
  42.0 0.1 reshape.113
  42.2 1.5 %fusion.15 = f32[96,256]{1,0:T(8,128)S(1)} fusion(bf16[96,2048]{1,0:T(8,128)(2,1)S(1)} %reshape.113, bf16[1,2048,256]{2,1,0:T(8,128)(2,1)} %param.33), kind=kOutput, calls=%fused_computation.24 | convolution fusion | flops 100663296 | bytes 1540096 | tf_op jit(solution)/shard_map/dot_general | solution.py:100
  43.7 1.5 %fusion.10 = bf16[96,256]{1,0:T(8,128)(2,1)S(1)} fusion(bf16[96,2048]{1,0:T(8,128)(2,1)S(1)} %reshape.113, bf16[1,2048,256]{2,1,0:T(8,128)(2,1)} %param.34, f32[96,256]{1,0:T(8,128)S(1)} %fusion.15), kind=kOutput, calls=%fused_computation.17 | convolution fusion | flops 100810752 | bytes 1589248 | tf_op jit(solution)/shard_map/dot_general | solution.py:101
  45.3 2.3 %convolution_convert_fusion = bf16[16,6,2048]{2,0,1:T(8,128)(2,1)} fusion(bf16[1,256,2048]{2,1,0:T(8,128)(2,1)} %param.35, bf16[16,6,256]{2,1,0:T(8,128)(2,1)S(1)} %dot_general.37), kind=kOutput, calls=%fused_computation.1 | convolution fusion | flops 100859904 | bytes 1490944 | tf_op jit(solution)/shard_map/dot_general | solution.py:103
  47.7 5.8 %reduce-scatter.2.cloned.1.call-done = bf16[16,6,1024]{2,0,1:T(8,128)(2,1)} async-done(((bf16[16,6,2048]{2,0,1:T(8,128)(2,1)}), bf16[16,6,1024]{2,0,1:T(8,128)(2,1)}) %reduce-scatter.2.cloned.1.call-update) | async-done | bytes 196624 | tf_op jit(solution)/shard_map/reduce_scatter | solution.py:106
  53.5 1.7 %copy.63 = bf16[16,6,1024]{2,1,0:T(8,128)(2,1)} copy(bf16[16,6,1024]{2,0,1:T(8,128)(2,1)} %reduce-scatter.2.cloned.1.call-done) | data formatting | bytes 393216 | tf_op jit(solution)/shard_map/reduce_scatter | solution.py:106
  55.2 6.7 %all-to-all-start.1 = ((bf16[16,6,1024]{2,1,0:T(8,128)(2,1)}), bf16[16,6,1024]{2,1,0:T(8,128)(2,1)S(1)}, u32[]{:S(2)}, u32[]{:S(2)}) async-start(bf16[16,6,1024]{2,1,0:T(8,128)(2,1)} %copy.63), calls=%async_computation.2 | async-start | bytes 524288 | tf_op jit(solution)/shard_map/all_to_all | solution.py:109
  62.1 0.1 mul.189
  62.2 0.1 copy.61
  62.4 9.9 %all-to-all-done.1 = bf16[16,6,1024]{2,1,0:T(8,128)(2,1)S(1)} async-done(((bf16[16,6,1024]{2,1,0:T(8,128)(2,1)}), bf16[16,6,1024]{2,1,0:T(8,128)(2,1)S(1)}, u32[]{:S(2)}, u32[]{:S(2)}) %all-to-all-start.1) | async-done | bytes 196640 | tf_op jit(solution)/shard_map/all_to_all | solution.py:109
  72.4 0.8 gather_fusion
  73.3 0.7 multiply_reduce_fusion
  74.0 0.7 add_convert_fusion
  (54 shorter events, 1.3 us)
Async XLA Ops:
  7.2 10.1 %copy-start = (bf16[1024,1024]{1,0:T(8,128)(2,1)S(1)}, bf16[1024,1024]{1,0:T(8,128)(2,1)}, u32[]{:S(2)}) copy-start(bf16[1024,1024]{1,0:T(8,128)(2,1)} %param.28) | copy-start | bytes 6291460
  7.2 4.8 %copy-start.3 = (bf16[48,3,512]{2,0,1:T(8,128)(2,1)S(1)}, bf16[48,3,512]{2,0,1:T(8,128)(2,1)}, u32[]{:S(2)}) copy-start(bf16[48,3,512]{2,0,1:T(8,128)(2,1)} %param.19) | copy-start | bytes 442372
  7.2 4.8 %copy-start.7 = (f32[4,512]{1,0:T(4,128)S(1)}, f32[4,512]{1,0:T(4,128)}, u32[]{:S(2)}) copy-start(f32[4,512]{1,0:T(4,128)} %param.24) | copy-start | bytes 24580
  7.2 5.0 %copy-start.12 = (bf16[8,64,64]{2,1,0:T(8,128)(2,1)S(1)}, bf16[8,64,64]{2,1,0:T(8,128)(2,1)}, u32[]{:S(2)}) copy-start(bf16[8,64,64]{2,1,0:T(8,128)(2,1)} %param.25) | copy-start | bytes 196612
  7.2 46.3 %reduce-scatter.2.cloned.1.call-start = ((), (), s32[]{:S(2)}) async-start(), calls=%async_computation.3 | async-start | bytes 589824 | tf_op jit(solution)/shard_map/reduce_scatter | solution.py:106
  9.8 2.8 %copy-start.13 = (bf16[8,64,64]{2,1,0:T(8,128)(2,1)S(1)}, bf16[8,64,64]{2,1,0:T(8,128)(2,1)}, u32[]{:S(2)}) copy-start(bf16[8,64,64]{2,1,0:T(8,128)(2,1)} %param.26) | copy-start | bytes 196612
  12.0 1.0 %copy-start.9 = (f32[512]{0:T(512)S(1)}, f32[512]{0:T(512)}, u32[]{:S(2)}) copy-start(f32[512]{0:T(512)} %param.27) | copy-start | bytes 6148
  12.0 1.0 %copy-start.4 = (f32[48,512]{1,0:T(8,128)S(1)}, f32[48,512]{1,0:T(8,128)}, u32[]{:S(2)}) copy-start(f32[48,512]{1,0:T(8,128)} %param.20) | copy-start | bytes 294916
  12.1 1.1 %copy-start.5 = (f32[2048]{0:T(1024)S(1)}, f32[2048]{0:T(1024)}, u32[]{:S(2)}) copy-start(f32[2048]{0:T(1024)} %param.21) | copy-start | bytes 24580
  12.8 4.4 %copy-start.1 = (bf16[48,1024]{1,0:T(8,128)(2,1)S(1)}, bf16[48,1024]{1,0:T(8,128)(2,1)}, u32[]{:S(2)}) copy-start(bf16[48,1024]{1,0:T(8,128)(2,1)} %param.18) | copy-start | bytes 294916
  13.2 4.7 %copy-start.2 = (f32[48,512]{1,0:T(8,128)}, f32[48,512]{1,0:T(8,128)S(1)}, u32[]{:S(2)}) copy-start(f32[48,512]{1,0:T(8,128)S(1)} %multiply_add_fusion) | copy-start | bytes 294916
  13.2 7.2 %copy-start.6 = (s32[48,2]{0,1:T(2,128)S(1)}, s32[48,2]{0,1:T(2,128)}, u32[]{:S(2)}) copy-start(s32[48,2]{0,1:T(2,128)} %param.30) | copy-start | bytes 1156
  15.4 5.9 %copy-start.8 = (f32[2048]{0:T(1024)S(1)}, f32[2048]{0:T(1024)}, u32[]{:S(2)}) copy-start(f32[2048]{0:T(1024)} %param.29) | copy-start | bytes 24580
  43.7 3.9 %copy-start.10 = (f32[48,2]{0,1:T(2,128)S(1)}, f32[48,2]{0,1:T(2,128)}, u32[]{:S(2)}) copy-start(f32[48,2]{0,1:T(2,128)} %param.32) | copy-start | bytes 1156
  43.7 3.9 %copy-start.11 = (f32[48]{0:T(128)S(1)}, f32[48]{0:T(128)}, u32[]{:S(2)}) copy-start(f32[48]{0:T(128)} %param.31) | copy-start | bytes 580
  55.2 17.1 %all-to-all-start.1 = ((bf16[16,6,1024]{2,1,0:T(8,128)(2,1)}), bf16[16,6,1024]{2,1,0:T(8,128)(2,1)S(1)}, u32[]{:S(2)}, u32[]{:S(2)}) async-start(bf16[16,6,1024]{2,1,0:T(8,128)(2,1)} %copy.63), calls=%async_computation.2 | async-start | bytes 524288 | tf_op jit(solution)/shard_map/all_to_all | solution.py:109
Sparse Core Ops, SparseCore 0:
  47.7 5.7 reduce-scatter.1
where the time goes:
time: 82 us; the launch traced here: 81.5 us
  blocking collectives  27.2 us (33%)
  waiting for transfers between devices  15.8 us (19%)
  between operations  14.4 us (18%)
  matrix products  10.9 us (13%)
  starting transfers between devices  6.77 us (8%)
  local copies, waits for them, and re-layouts  4.27 us (5%)
  other arithmetic  2.18 us (3%)
    all_to_all x1, blocking collectives, local(): lax.all_to_all(outgoing, 'ep', split_axis=0, concat_axis=0, tiled=True)  18.2 us
    all_to_all x1, waiting for transfers between devices, local(): lax.all_to_all(summed, 'ep', split_axis=0, concat_axis=0, tiled=True)  9.95 us
    all_to_all x1, starting transfers between devices, local(): lax.all_to_all(summed, 'ep', split_axis=0, concat_axis=0, tiled=True)  6.73 us
    reduce_scatter x1, waiting for transfers between devices, local(): lax.psum_scatter(partial_value.astype(jnp.bfloat16), 'tp', scatter_dimens...  5.84 us
    psum x1, blocking collectives, local(): square_total = lax.psum(jnp.sum(values * values, axis=1), 'tp')  2.49 us
    all_gather x1, blocking collectives, local(): whole_tokens = lax.all_gather(tokens, 'tp', axis=1, tiled=True)  2.42 us
    dot_general x1, matrix products, local(): jnp.dot(hidden_units, expert_down[0], preferred_element_type=jnp.float32)  2.27 us
    dot_general x1, matrix products, local(): jnp.dot(normed, gelu_weight, preferred_element_type=jnp.float32)  2.18 us
  transfers between devices with their start and end apart: 2, of which 2 were waited for; matrix products, arithmetic and copies ran while one was open for 1% of the time, Pallas kernels for 0%

commit v1 on v0

--- a/solution.py
+++ b/solution.py
@@ -81,7 +81,9 @@
     )
     values = residual.astype(jnp.float32)
     half_width = values.shape[1]
-    square_total = lax.psum(jnp.sum(values * values, axis=1), "tp")
+    original = jnp.sum(values * values, axis=1)
+    top = lax.all_gather(original, "tp")
+    square_total = jnp.sum(top, axis=0)
     gain_part = lax.dynamic_slice_in_dim(
         expert_gain, lax.axis_index("tp") * half_width, half_width, 0
     )

time: 82 us -> 83.6 us (1.020)
  local copies, waits for them, and re-layouts: 4.27 us -> 5.18 us
    psum x1 -> x0, blocking collectives: 2.49 us -> none  [local(): square_total = lax.psum(jnp.sum(values * values, axis=1), 'tp')]
    unnamed x0 -> x1, blocking collectives: none -> 2.46 us
where the time goes in v1:
time: 83.6 us; the launch traced here: 83.1 us
  blocking collectives  27.1 us (32%)
  waiting for transfers between devices  15.8 us (19%)
  between operations  15.1 us (18%)
  matrix products  10.9 us (13%)
  starting transfers between devices  6.77 us (8%)
  local copies, waits for them, and re-layouts  5.18 us (6%)
  other arithmetic  2.2 us (3%)
    all_to_all x1, blocking collectives, local(): lax.all_to_all(outgoing, 'ep', split_axis=0, concat_axis=0, tiled=True)  18.2 us
    all_to_all x1, waiting for transfers between devices, local(): lax.all_to_all(summed, 'ep', split_axis=0, concat_axis=0, tiled=True)  9.95 us
    all_to_all x1, starting transfers between devices, local(): lax.all_to_all(summed, 'ep', split_axis=0, concat_axis=0, tiled=True)  6.73 us
    reduce_scatter x1, waiting for transfers between devices, local(): lax.psum_scatter(partial_value.astype(jnp.bfloat16), 'tp', scatter_dimens...  5.84 us
    unnamed x1, blocking collectives  2.46 us
    all_gather x1, blocking collectives, local(): whole_tokens = lax.all_gather(tokens, 'tp', axis=1, tiled=True)  2.42 us
    dot_general x1, matrix products, local(): jnp.dot(hidden_units, expert_down[0], preferred_element_type=jnp.float32)  2.27 us
    dot_general x1, matrix products, local(): jnp.dot(normed, gelu_weight, preferred_element_type=jnp.float32)  2.18 us
  transfers between devices with their start and end apart: 2, of which 2 were waited for; matrix products, arithmetic and copies ran while one was open for 1% of the time, Pallas kernels for 0%

profile of v1, /device:TPU:0, one launch (start us, length us, event | category | flops | bytes accessed | tf_op | source)
XLA Modules:
  0.0 83.1 jit_solution(5435171774232731353)
XLA Ops:
  7.3 2.4 %all_gather.15 = bf16[48,2048]{1,0:T(8,128)(2,1)S(1)} all-gather(bf16[48,1024]{1,0:T(8,128)(2,1)} %param.18), channel_id=1, replica_groups=mesh['ep'=16,'tp'=2] {'tp'}, dimensions={1}, use_global_device_ids=true | all-gather | bytes 294912 | tf_op jit(solution)/shard_map/all_gather | solution.py:35
  9.7 0.1 fusion.17
  9.9 2.2 %fusion.12 = bf16[48,1,512]{2,0,1:T(8,128)(2,1)S(1)} fusion(bf16[2048,512]{1,0:T(8,128)(2,1)} %param.22, bf16[48,2048]{1,0:T(8,128)(2,1)S(1)} %all_gather.15, f32[2048]{0:T(1024)} %param.21, f32[48]{0:T(128)S(1)} %add_rsqrt_fusion.1), kind=kOutput, calls=%fused_computation.21 | convolution fusion | flops 101081088 | bytes 2351296 | tf_op jit(solution)/shard_map/dot_general | solution.py:37
  12.1 0.1 convert_element_type.75
  12.3 0.2 fusion.7
  12.6 0.2 fusion.3
  13.2 2.2 %fusion.28 = bf16[48,512]{1,0:T(8,128)(2,1)S(1)} fusion(f32[48,512]{1,0:T(8,128)S(1)} %multiply_add_fusion, bf16[2048,512]{1,0:T(8,128)(2,1)} %param.23, bf16[48,2048]{1,0:T(8,128)(2,1)S(1)} %all_gather.15, f32[2048]{0:T(1024)S(1)} %copy-done.5, f32[48]{0:T(128)S(1)} %add_rsqrt_fusion.1), kind=kOutput, calls=%fused_computation.46 | convolution fusion | flops 101351424 | bytes 2449600 | tf_op jit(solution)/shard_map/dot_general | solution.py:38
  15.4 1.9 %all_gather.16 = bf16[48,1024]{1,0:T(8,128)(2,1)S(1)} all-gather(bf16[48,512]{1,0:T(8,128)(2,1)S(1)} %fusion.28), channel_id=1, replica_groups=mesh['ep'=16,'tp'=2] {'tp'}, dimensions={1}, use_global_device_ids=true | all-gather | bytes 147456 | tf_op jit(solution)/shard_map/all_gather | solution.py:61
  17.3 0.6 multiply_reduce_fusion.2
  17.9 0.6 dynamic-slice
  19.2 0.2 dynamic-update-slice
  19.4 2.5 %all-reduce = f32[96]{0:T(128)S(1)} all-reduce(f32[96]{0:T(128)S(1)} %dynamic-update-slice), channel_id=2, replica_groups=mesh['ep'=16,'tp'=2] {'tp'}, use_global_device_ids=true, to_apply=%add | all-reduce | flops 96 | bytes 768
  22.1 0.1 reshape.115
  22.3 0.1 reduce_window_sum.11
  22.4 0.2 select_reduce_fusion
  22.6 0.1 reduce_sum.80
  23.0 0.3 convolution_convert_fusion.1
  23.3 18.2 %all_to_all.10 = bf16[16,6,1024]{2,1,0:T(8,128)(2,1)S(1)} all-to-all(bf16[16,6,1024]{2,1,0:T(8,128)(2,1)S(1)} %reshape.116), channel_id=1, replica_groups=mesh['ep'=16,'tp'=2] {'ep'}, dimensions={0} | all-to-all | bytes 393216 | tf_op jit(solution)/shard_map/all_to_all | solution.py:95
  41.5 2.2 %all_gather.19 = bf16[16,6,2048]{2,1,0:T(8,128)(2,1)S(1)} all-gather(bf16[16,6,1024]{2,1,0:T(8,128)(2,1)S(1)} %all_to_all.10), channel_id=1, replica_groups=mesh['ep'=16,'tp'=2] {'tp'}, dimensions={2}, use_global_device_ids=true | all-gather | bytes 589824 | tf_op jit(solution)/shard_map/all_gather | solution.py:94
  43.7 0.1 reshape.117
  43.8 1.5 %fusion.15 = f32[96,256]{1,0:T(8,128)S(1)} fusion(bf16[96,2048]{1,0:T(8,128)(2,1)S(1)} %reshape.117, bf16[1,2048,256]{2,1,0:T(8,128)(2,1)} %param.33), kind=kOutput, calls=%fused_computation.24 | convolution fusion | flops 100663296 | bytes 1540096 | tf_op jit(solution)/shard_map/dot_general | solution.py:102
  45.4 1.5 %fusion.10 = bf16[96,256]{1,0:T(8,128)(2,1)S(1)} fusion(bf16[96,2048]{1,0:T(8,128)(2,1)S(1)} %reshape.117, bf16[1,2048,256]{2,1,0:T(8,128)(2,1)} %param.34, f32[96,256]{1,0:T(8,128)S(1)} %fusion.15), kind=kOutput, calls=%fused_computation.17 | convolution fusion | flops 100810752 | bytes 1589248 | tf_op jit(solution)/shard_map/dot_general | solution.py:103
  46.9 2.3 %convolution_convert_fusion = bf16[16,6,2048]{2,0,1:T(8,128)(2,1)} fusion(bf16[1,256,2048]{2,1,0:T(8,128)(2,1)} %param.35, bf16[16,6,256]{2,1,0:T(8,128)(2,1)S(1)} %dot_general.37), kind=kOutput, calls=%fused_computation.1 | convolution fusion | flops 100859904 | bytes 1490944 | tf_op jit(solution)/shard_map/dot_general | solution.py:105
  49.3 5.8 %reduce-scatter.2.cloned.1.call-done = bf16[16,6,1024]{2,0,1:T(8,128)(2,1)} async-done(((bf16[16,6,2048]{2,0,1:T(8,128)(2,1)}), bf16[16,6,1024]{2,0,1:T(8,128)(2,1)}) %reduce-scatter.2.cloned.1.call-update) | async-done | bytes 196624 | tf_op jit(solution)/shard_map/reduce_scatter | solution.py:108
  55.1 1.7 %copy.63 = bf16[16,6,1024]{2,1,0:T(8,128)(2,1)} copy(bf16[16,6,1024]{2,0,1:T(8,128)(2,1)} %reduce-scatter.2.cloned.1.call-done) | data formatting | bytes 393216 | tf_op jit(solution)/shard_map/reduce_scatter | solution.py:108
  56.8 6.7 %all-to-all-start.1 = ((bf16[16,6,1024]{2,1,0:T(8,128)(2,1)}), bf16[16,6,1024]{2,1,0:T(8,128)(2,1)S(1)}, u32[]{:S(2)}, u32[]{:S(2)}) async-start(bf16[16,6,1024]{2,1,0:T(8,128)(2,1)} %copy.63), calls=%async_computation.2 | async-start | bytes 524288 | tf_op jit(solution)/shard_map/all_to_all | solution.py:111
  63.7 0.1 mul.189
  63.8 0.1 copy.61
  64.0 9.9 %all-to-all-done.1 = bf16[16,6,1024]{2,1,0:T(8,128)(2,1)S(1)} async-done(((bf16[16,6,1024]{2,1,0:T(8,128)(2,1)}), bf16[16,6,1024]{2,1,0:T(8,128)(2,1)S(1)}, u32[]{:S(2)}, u32[]{:S(2)}) %all-to-all-start.1) | async-done | bytes 196640 | tf_op jit(solution)/shard_map/all_to_all | solution.py:111
  74.1 0.8 gather_fusion
  74.9 0.7 multiply_reduce_fusion
  75.6 0.7 add_convert_fusion
  (61 shorter events, 1.6 us)
Async XLA Ops:
  7.2 10.1 %copy-start = (bf16[1024,1024]{1,0:T(8,128)(2,1)S(1)}, bf16[1024,1024]{1,0:T(8,128)(2,1)}, u32[]{:S(2)}) copy-start(bf16[1024,1024]{1,0:T(8,128)(2,1)} %param.28) | copy-start | bytes 6291460
  7.2 4.8 %copy-start.3 = (bf16[48,3,512]{2,0,1:T(8,128)(2,1)S(1)}, bf16[48,3,512]{2,0,1:T(8,128)(2,1)}, u32[]{:S(2)}) copy-start(bf16[48,3,512]{2,0,1:T(8,128)(2,1)} %param.19) | copy-start | bytes 442372
  7.2 4.8 %copy-start.7 = (f32[4,512]{1,0:T(4,128)S(1)}, f32[4,512]{1,0:T(4,128)}, u32[]{:S(2)}) copy-start(f32[4,512]{1,0:T(4,128)} %param.24) | copy-start | bytes 24580
  7.2 5.0 %copy-start.12 = (bf16[8,64,64]{2,1,0:T(8,128)(2,1)S(1)}, bf16[8,64,64]{2,1,0:T(8,128)(2,1)}, u32[]{:S(2)}) copy-start(bf16[8,64,64]{2,1,0:T(8,128)(2,1)} %param.25) | copy-start | bytes 196612
  7.2 47.9 %reduce-scatter.2.cloned.1.call-start = ((), (), s32[]{:S(2)}) async-start(), calls=%async_computation.3 | async-start | bytes 589824 | tf_op jit(solution)/shard_map/reduce_scatter | solution.py:108
  9.8 2.8 %copy-start.13 = (bf16[8,64,64]{2,1,0:T(8,128)(2,1)S(1)}, bf16[8,64,64]{2,1,0:T(8,128)(2,1)}, u32[]{:S(2)}) copy-start(bf16[8,64,64]{2,1,0:T(8,128)(2,1)} %param.26) | copy-start | bytes 196612
  12.0 1.0 %copy-start.9 = (f32[512]{0:T(512)S(1)}, f32[512]{0:T(512)}, u32[]{:S(2)}) copy-start(f32[512]{0:T(512)} %param.27) | copy-start | bytes 6148
  12.1 1.0 %copy-start.4 = (f32[48,512]{1,0:T(8,128)S(1)}, f32[48,512]{1,0:T(8,128)}, u32[]{:S(2)}) copy-start(f32[48,512]{1,0:T(8,128)} %param.20) | copy-start | bytes 294916
  12.1 1.1 %copy-start.5 = (f32[2048]{0:T(1024)S(1)}, f32[2048]{0:T(1024)}, u32[]{:S(2)}) copy-start(f32[2048]{0:T(1024)} %param.21) | copy-start | bytes 24580
  12.9 4.5 %copy-start.1 = (bf16[48,1024]{1,0:T(8,128)(2,1)S(1)}, bf16[48,1024]{1,0:T(8,128)(2,1)}, u32[]{:S(2)}) copy-start(bf16[48,1024]{1,0:T(8,128)(2,1)} %param.18) | copy-start | bytes 294916
  13.2 4.7 %copy-start.2 = (f32[48,512]{1,0:T(8,128)}, f32[48,512]{1,0:T(8,128)S(1)}, u32[]{:S(2)}) copy-start(f32[48,512]{1,0:T(8,128)S(1)} %multiply_add_fusion) | copy-start | bytes 294916
  13.2 4.7 %copy-start.14 = (u32[32]{0:T(128)S(1)}, u32[32]{0:T(128)}, u32[]{:S(2)}) copy-start(u32[32]{0:T(128)} %constant.60) | copy-start | bytes 388
  13.2 8.8 %copy-start.6 = (s32[48,2]{0,1:T(2,128)S(1)}, s32[48,2]{0,1:T(2,128)}, u32[]{:S(2)}) copy-start(s32[48,2]{0,1:T(2,128)} %param.30) | copy-start | bytes 1156
  15.4 7.5 %copy-start.8 = (f32[2048]{0:T(1024)S(1)}, f32[2048]{0:T(1024)}, u32[]{:S(2)}) copy-start(f32[2048]{0:T(1024)} %param.29) | copy-start | bytes 24580
  45.3 3.9 %copy-start.10 = (f32[48,2]{0,1:T(2,128)S(1)}, f32[48,2]{0,1:T(2,128)}, u32[]{:S(2)}) copy-start(f32[48,2]{0,1:T(2,128)} %param.32) | copy-start | bytes 1156
  45.3 3.9 %copy-start.11 = (f32[48]{0:T(128)S(1)}, f32[48]{0:T(128)}, u32[]{:S(2)}) copy-start(f32[48]{0:T(128)} %param.31) | copy-start | bytes 580
  56.8 17.1 %all-to-all-start.1 = ((bf16[16,6,1024]{2,1,0:T(8,128)(2,1)}), bf16[16,6,1024]{2,1,0:T(8,128)(2,1)S(1)}, u32[]{:S(2)}, u32[]{:S(2)}) async-start(bf16[16,6,1024]{2,1,0:T(8,128)(2,1)} %copy.63), calls=%async_computation.2 | async-start | bytes 524288 | tf_op jit(solution)/shard_map/all_to_all | solution.py:111
Sparse Core Ops, SparseCore 0:
  49.3 5.7 reduce-scatter.1
